TPU v7x, 32 devices: a whole 2x2x4 slice. The times are simulated.
32 devices in a mesh: grp: 2 (over x), ep: 8 (over z, y), tp: 2 (over core).
Axes of the slice: x: 2, y: 2, z: 4, core: 2. Of those that a mesh axis runs over, the one named last changes fastest.
Arguments:
- hidden_in: bfloat16 [256, 2048], P(('grp', 'ep', 'tp')), parts along dimension 0, may hold values from -6 to 6
- query_nope: bfloat16 [256, 16, 64], P(('grp', 'ep', 'tp')), parts along dimension 0, may hold values from -102 to 102
- query_rope: bfloat16 [256, 16, 32], P(('grp', 'ep', 'tp')), parts along dimension 0, may hold values from -6 to 6
- new_latent: bfloat16 [256, 256], P(('grp', 'ep', 'tp')), parts along dimension 0, may hold values from -6 to 6
- new_rope: bfloat16 [256, 32], P(('grp', 'ep', 'tp')), parts along dimension 0, may hold values from -6 to 6
- cache_latent: bfloat16 [256, 1024, 256], P(('grp', 'ep', 'tp')), parts along dimension 0, may hold values from -6 to 6
- cache_rope: bfloat16 [256, 1024, 32], P(('grp', 'ep', 'tp')), parts along dimension 0, may hold values from -6 to 6
- lengths: int32 [256], P(('grp', 'ep', 'tp')), parts along dimension 0, may hold values from 1 to 1024, as said below
- absorb_key: bfloat16 [256, 16, 64], replicated, may hold values from -0.75 to 0.75
- value_up: bfloat16 [256, 16, 128], replicated, may hold values from -0.375 to 0.375
- out_proj: bfloat16 [2048, 2048], P(None, ('ep', 'tp')), may hold values from -0.125 to 0.125
- gain_mix: bfloat16 [2048], replicated, may hold values from 0.099609375 to 1.8984375
- gain_ffn_in: bfloat16 [2048], replicated, may hold values from 0.099609375 to 1.8984375
- router: bfloat16 [2048, 16], replicated, may hold values from -0.125 to 0.125
- routes: int32 [256, 6], P(('grp', 'ep')), parts along dimension 0, may hold values from 0 to 15, all different within a row; in each aligned block of 16 rows (0 to 15, 16 to 31, ...) at most 12 rows name the same one
- expert_gate: bfloat16 [16, 2048, 256], P(('ep', 'tp')), may hold values from -0.125 to 0.125
- expert_up: bfloat16 [16, 2048, 256], P(('ep', 'tp')), may hold values from -0.125 to 0.125
- expert_down: bfloat16 [16, 256, 2048], P(('ep', 'tp')), may hold values from -0.375 to 0.375
- shared_gate: bfloat16 [2048, 256], replicated, may hold values from -0.125 to 0.125
- shared_up: bfloat16 [2048, 256], replicated, may hold values from -0.125 to 0.125
- shared_down: bfloat16 [256, 2048], replicated, may hold values from -0.375 to 0.375
- gain_ffn_out: bfloat16 [2048], replicated, may hold values from 0.099609375 to 1.8984375
Outputs:
- layer_out: bfloat16 [256, 2048], P(('grp', 'ep', 'tp')), parts along dimension 0
There are 2 independent parts, one for each index of `grp`. A program takes and returns all parts, laid end to end along the dimension named above; an argument that names none is the same for every part. Nothing has to cross between parts.
Inputs may be any that keep to these rules, and one draw needn't show every extreme that they name: `lengths`: every sequence holds 1 to 1024 cached positions, and some sequence holds 1024. `routes`: each row names 6 different experts; in each aligned block of 16 rows (the rows of one index of ep) no expert is named by more than 12 rows, and in some block some expert is named by exactly 12 rows.
All inputs are finite; a program needn't handle non-finite values.
Results may differ from a plain program's by a relative error of at most 0.015.
Values may be sent and summed in bfloat16 or wider, within the bound.
A program may use at most 64 MiB of HBM per device.

v0:
```python
import jax
import jax.numpy as jnp
from jax import lax
from jax.sharding import PartitionSpec as P

ABLK = 512


rope_theta = 10000.0
norm_eps = 1e-06
routed_scale = 2.5
masked_score = -1e30


def normalize(values):
    return values * lax.rsqrt(jnp.mean(values * values, axis=-1, keepdims=True) + norm_eps)


def rotate(values, positions):
    half_dim = values.shape[-1] // 2
    inverse = rope_theta ** (-jnp.arange(half_dim, dtype=jnp.float32) * 2.0 / values.shape[-1])
    angles = positions * inverse
    cosine = jnp.cos(angles)
    sine_table = jnp.sin(angles)
    first_half = values[..., :half_dim]
    second_half = values[..., half_dim:]
    return jnp.concatenate(
        [
            first_half * cosine - second_half * sine_table,
            first_half * sine_table + second_half * cosine,
        ],
        axis=-1,
    )


def swiglu(flat_rows, gate_w, up_w, down_w):
    gate_part = jnp.dot(flat_rows, gate_w, preferred_element_type=jnp.float32)
    up_part = jnp.dot(flat_rows, up_w, preferred_element_type=jnp.float32)
    inner_rows = (jax.nn.silu(gate_part) * up_part).astype(jnp.bfloat16)
    return jnp.dot(inner_rows, down_w, preferred_element_type=jnp.float32).astype(jnp.bfloat16)


def local(
    hidden_in,
    query_nope,
    query_rope,
    new_latent,
    new_rope,
    cache_latent,
    cache_rope,
    lengths,
    absorb_key,
    value_up,
    out_proj,
    gain_mix,
    gain_ffn_in,
    router,
    routes,
    expert_gate,
    expert_up,
    expert_down,
    shared_gate,
    shared_up,
    shared_down,
    gain_ffn_out,
):
    seq_count = hidden_in.shape[0]
    positions = lengths.astype(jnp.float32)
    query_latent = jnp.einsum(
        "shn,chn->shc", query_nope, absorb_key, preferred_element_type=jnp.float32
    ).astype(jnp.bfloat16)
    query_pe = rotate(query_rope.astype(jnp.float32), positions[:, None, None]).astype(jnp.bfloat16)
    latent_new = normalize(new_latent.astype(jnp.float32)).astype(jnp.bfloat16)
    key_new = rotate(new_rope.astype(jnp.float32), positions[:, None]).astype(jnp.bfloat16)
    score_scale = (query_nope.shape[-1] + query_rope.shape[-1]) ** (-0.5)
    new_score = (
        jnp.einsum("shc,sc->sh", query_latent, latent_new, preferred_element_type=jnp.float32)
        + jnp.einsum("shr,sr->sh", query_pe, key_new, preferred_element_type=jnp.float32)
    ) * score_scale

    def attend_block(block_index, loop_state):
        running_max, weight_total, weighted_sum = loop_state
        block_start = block_index * ABLK
        block_latent = lax.dynamic_slice_in_dim(cache_latent, block_start, ABLK, 1)
        block_rope = lax.dynamic_slice_in_dim(cache_rope, block_start, ABLK, 1)
        scores = (
            jnp.einsum(
                "shc,skc->shk", query_latent, block_latent, preferred_element_type=jnp.float32
            )
            + jnp.einsum("shr,skr->shk", query_pe, block_rope, preferred_element_type=jnp.float32)
        ) * score_scale
        key_index = block_start + lax.iota(jnp.int32, ABLK)
        in_range = key_index[None, None, :] < lengths[:, None, None]
        scores = jnp.where(in_range, scores, masked_score)
        new_max = jnp.maximum(running_max, jnp.max(scores, axis=-1))
        rescale = jnp.exp(running_max - new_max)
        weights = jnp.exp(scores - new_max[..., None])
        weight_total = weight_total * rescale + jnp.sum(weights, axis=-1)
        weighted_sum = weighted_sum * rescale[..., None] + jnp.einsum(
            "shk,skc->shc",
            weights.astype(jnp.bfloat16),
            block_latent,
            preferred_element_type=jnp.float32,
        )
        return (new_max, weight_total, weighted_sum)

    longest = jnp.max(lengths)
    block_count = (longest + ABLK - 1) // ABLK
    ones_start = jnp.ones_like(new_score)
    sum_start = ones_start[..., None] * latent_new.astype(jnp.float32)[:, None, :]
    final_max, weight_total, weighted_sum = lax.fori_loop(
        0, block_count, attend_block, (new_score, ones_start, sum_start)
    )
    latent_out = (weighted_sum / weight_total[..., None]).astype(jnp.bfloat16)
    heads_out = (
        jnp.einsum("shc,chv->shv", latent_out, value_up, preferred_element_type=jnp.float32)
        .astype(jnp.bfloat16)
        .reshape(seq_count, -1)
    )
    column_rows = jnp.dot(
        lax.all_gather(heads_out, ("ep", "tp"), axis=0, tiled=True),
        out_proj,
        preferred_element_type=jnp.float32,
    ).astype(jnp.bfloat16)
    mixed_rows = lax.all_to_all(column_rows, ("ep", "tp"), split_axis=0, concat_axis=1, tiled=True)
    after_mix = (
        hidden_in.astype(jnp.float32)
        + gain_mix.astype(jnp.float32) * normalize(mixed_rows.astype(jnp.float32))
    ).astype(jnp.bfloat16)
    ffn_in = (normalize(after_mix.astype(jnp.float32)) * gain_ffn_in.astype(jnp.float32)).astype(
        jnp.bfloat16
    )
    affinity = jax.nn.sigmoid(jnp.dot(ffn_in, router, preferred_element_type=jnp.float32))
    experts_total = router.shape[1]
    own_start = lax.axis_index("tp") * seq_count
    own_routes = lax.dynamic_slice_in_dim(routes, own_start, seq_count, 0)
    choose = own_routes[..., None] == lax.iota(jnp.int32, experts_total)[None, None, :]
    chosen = jnp.sum(jnp.where(choose, affinity[:, None, :], 0.0), axis=-1)
    route_weights = chosen / jnp.sum(chosen, axis=-1, keepdims=True) * routed_scale
    group_rows, top_count = routes.shape
    capacity = 2 * ((group_rows * top_count + experts_total - 1) // experts_total)
    flat_routes = routes.reshape(-1)
    order_index = lax.iota(jnp.int32, group_rows * top_count)
    same_expert = flat_routes[:, None] == flat_routes[None, :]
    earlier = order_index[None, :] < order_index[:, None]
    slot_number = jnp.sum(jnp.logical_and(same_expert, earlier), axis=1)
    slot_number = slot_number.reshape(group_rows, top_count)
    own_slots = lax.dynamic_slice_in_dim(slot_number, own_start, seq_count, 0)
    slot_index = own_routes * capacity + own_slots
    slots_total = experts_total * capacity
    slot_table = jnp.any(
        slot_index[None, :, :] == lax.iota(jnp.int32, slots_total)[:, None, None], axis=-1
    ).astype(jnp.bfloat16)
    outgoing_terms = jnp.dot(slot_table, ffn_in, preferred_element_type=jnp.float32)
    outgoing = outgoing_terms.astype(jnp.bfloat16).reshape(experts_total, capacity, -1)
    received = lax.all_to_all(outgoing, ("ep", "tp"), split_axis=0, concat_axis=0, tiled=True)
    ep_count = lax.axis_size("ep")
    tp_count = lax.axis_size("tp")
    item_count = received.shape[1]
    width = received.shape[2]
    merged = jnp.sum(received.reshape(ep_count, tp_count, item_count, width), axis=1)
    outputs = swiglu(
        merged.reshape(ep_count * item_count, width), expert_gate[0], expert_up[0], expert_down[0]
    )
    copies = jnp.broadcast_to(
        outputs.reshape(ep_count, 1, item_count, width), (ep_count, tp_count, item_count, width)
    )
    copies = copies.reshape(ep_count * tp_count, item_count, width)
    returned = lax.all_to_all(copies, ("ep", "tp"), split_axis=0, concat_axis=0, tiled=True)
    picked = returned.reshape(slots_total, -1)[slot_index]
    routed = jnp.sum(picked.astype(jnp.float32) * route_weights[..., None], axis=1)
    shared = swiglu(ffn_in, shared_gate, shared_up, shared_down)
    combined = routed + shared.astype(jnp.float32)
    return (
        after_mix.astype(jnp.float32) + gain_ffn_out.astype(jnp.float32) * normalize(combined)
    ).astype(jnp.bfloat16)


def solution(mesh):
    placed = (
        P(("grp", "ep", "tp"), None),
        P(("grp", "ep", "tp"), None, None),
        P(("grp", "ep", "tp"), None, None),
        P(("grp", "ep", "tp"), None),
        P(("grp", "ep", "tp"), None),
        P(("grp", "ep", "tp"), None, None),
        P(("grp", "ep", "tp"), None, None),
        P(("grp", "ep", "tp")),
        P(),
        P(),
        P(None, ("ep", "tp")),
        P(),
        P(),
        P(),
        P(("grp", "ep"), None),
        P(("ep", "tp"), None, None),
        P(("ep", "tp"), None, None),
        P(("ep", "tp"), None, None),
        P(),
        P(),
        P(),
        P(),
    )
    return jax.shard_map(
        local, mesh=mesh, in_specs=placed, out_specs=P(("grp", "ep", "tp"), None), check_vma=False
    )
```

profile of v0, /device:TPU:0, one launch (start us, length us, event | category | flops | bytes accessed | tf_op | source)
XLA Modules:
  0.0 117.5 jit_solution(18089685162042112679)
XLA Ops:
  0.0 1.4 %fusion.78 = (s32[]{:T(128)}, f32[8]{0:T(128)S(1)}) fusion(s32[8]{0:T(128)} %param.31), kind=kLoop, calls=%fused_computation.120 | loop fusion | flops 15 | bytes 68 | tf_op jit(solution)/shard_map/reduce_max | solution.py:107
  2.8 0.8 convert_element_type.112
  3.5 0.8 fusion.53
  4.3 0.8 fusion.65
  5.1 1.2 %fusion.21 = bf16[8,16,256]{2,0,1:T(8,128)(2,1)S(1)} fusion(bf16[256,16,64]{0,2,1:T(8,128)(2,1)} %param.32, bf16[8,16,64]{2,1,0:T(8,128)(2,1)} %param.25), kind=kOutput, calls=%fused_computation.30 | convolution fusion | flops 4227072 | bytes 606208 | tf_op jit(solution)/shard_map/shn,chn->shc/dot_general | solution.py:69
  7.1 6.6 %while.14 = (s32[]{:T(128)}, f32[8,16]{1,0:T(8,128)S(1)}, f32[8,16]{1,0:T(8,128)S(1)}, f32[8,16,256]{2,1,0:T(8,128)S(1)}, s32[]{:T(128)}, /*index=5*/s32[8]{0:T(...) while((s32[]{:T(128)}, f32[8,16]{1,0:T(8,128)S(1)}, ...), condition=%wide.region_5.6_spmd, body=%wide.region_2.5_spmd.sunk | while | flops 71897856 | bytes 6123747 | solution.py:111
  7.1 2.3 %fusion.108 = f32[8,512,16]{1,2,0:T(8,128)S(1)} fusion(bf16[8,16,256]{2,1,0:T(8,128)(2,1)S(1)} %get-tuple-element.239, bf16[8,1024,256]{2,1,0:T(8,128)(2,1)} %get-tuple-element.238, s32[]{:T(128)S(6)} %select_n.38), kind=kOutput, calls=%fused_computation.3.clone.1 | convolution fusion | flops 33554432 | bytes 2424836 | tf_op jit(solution)/shard_map/while/body/shc,skc->shk/dot_general | solution.py:87
  9.5 0.7 broadcast_compare_fusion.2
  10.2 1.2 %fusion.109 = (f32[8,16]{1,0:T(8,128)S(1)}, f32[8,16,512]{2,1,0:T(8,128)S(1)}) fusion(f32[8,512,16]{1,2,0:T(8,128)S(1)} %fusion.108, bf16[8,16,32]{2,1,0:T(8,128)(2,1)S(1)} %get-tuple-element.241, bf16[8,1024,32]{1,2,0:T(8,128)(2,1)} %get-tuple-element.240, s32[]{:T(128)S(6)} %select_n.38, pred[8,512]{1,0:T(8,128)(4,1)S(1)} %broadcast_compare_fusion.2), kind=kOutput, calls=%fused_computation.119.clone.1 | convolution fusion | flops 4456320 | bytes 799236 | tf_op jit(solution)/shard_map/while/body/shr,skr->shk/dot_general | solution.py:90
  11.6 2.0 %fusion.111 = f32[8,16,256]{2,1,0:T(8,128)S(1)} fusion(bf16[8,1024,256]{2,1,0:T(8,128)(2,1)} %get-tuple-element.238, s32[]{:T(128)S(6)} %select_n.38, f32[8,16,512]{2,1,0:T(8,128)S(1)} %get-tuple-element.201, f32[8,16,256]{2,1,0:T(8,128)S(1)} %get-tuple-element.221, f32[8,16]{1,0:T(8,128)S(1)} %max.4, f32[8,16]{1,0:T(8,128)S(1)} %get-tuple-element.203), kind=kOutput, calls=%fused_computation.9.clone.1 | convolution fusion | flops 33751040 | bytes 2622468 | tf_op jit(solution)/shard_map/while/body/shk,skc->shc/dot_general | solution.py:99
  14.1 28.0 %all_gather.3 = bf16[128,2048]{1,0:T(8,128)(2,1)S(1)} all-gather(bf16[8,2048]{1,0:T(8,128)(2,1)S(1)} %fusion.22), channel_id=1, replica_groups=mesh['grp'=2,'ep'=8,'tp'=2] {'ep','tp'}, dimensions={0}, use_global_device_ids=true | all-gather | bytes 557056 | tf_op jit(solution)/shard_map/all_gather | solution.py:121
  42.1 0.9 fusion.23
  43.0 3.5 %all-to-all-start = ((bf16[16,8,128]{2,1,0:T(8,128)(2,1)}), bf16[16,8,128]{2,1,0:T(8,128)(2,1)S(1)}, u32[]{:S(2)}, u32[]{:S(2)}) async-start(bf16[16,8,128]{2,1,0:T(8,128)(2,1)} %fusion.23), calls=%async_computation | async-start | bytes 65536 | tf_op jit(solution)/shard_map/all_to_all | solution.py:125
  47.2 5.9 %all-to-all-done = bf16[16,8,128]{2,1,0:T(8,128)(2,1)S(1)} async-done(((bf16[16,8,128]{2,1,0:T(8,128)(2,1)}), bf16[16,8,128]{2,1,0:T(8,128)(2,1)S(1)}, u32[]{:S(2)}, u32[]{:S(2)}) %all-to-all-start) | async-done | bytes 32800 | tf_op jit(solution)/shard_map/all_to_all | solution.py:125
  54.1 27.4 %all_to_all.23 = bf16[16,12,2048]{2,1,0:T(8,128)(2,1)S(1)} all-to-all(bf16[16,12,2048]{2,1,0:T(8,128)(2,1)S(1)} %reshape.193), channel_id=1, replica_groups=mesh['grp'=2,'ep'=8,'tp'=2] {'ep','tp'}, dimensions={0} | all-to-all | bytes 1572864 | tf_op jit(solution)/shard_map/all_to_all | solution.py:156
  81.8 1.6 %fusion.31 = f32[96,256]{1,0:T(8,128)S(1)} fusion(bf16[96,2048]{1,0:T(8,128)(2,1)S(1)} %reshape.195, bf16[1,2048,256]{2,1,0:T(8,128)(2,1)} %param.39), kind=kOutput, calls=%fused_computation.43 | convolution fusion | flops 100663296 | bytes 1540096 | tf_op jit(solution)/shard_map/dot_general | solution.py:37
  83.4 0.8 convolution_convert_fusion.1
  84.3 1.1 broadcast_in_dim.31
  85.4 4.9 %all-to-all-start.2 = ((bf16[16,12,2048]{2,1,0:T(8,128)(2,1)}), bf16[16,12,2048]{2,1,0:T(8,128)(2,1)S(1)}, u32[]{:S(2)}, u32[]{:S(2)}) async-start(bf16[16,12,2048]{2,1,0:T(8,128)(2,1)} %bitcast.17), calls=%async_computation.2 | async-start | bytes 2097152 | tf_op jit(solution)/shard_map/all_to_all | solution.py:169
  91.0 1.5 %fusion.72 = f32[8,256]{1,0:T(8,128)S(1)} fusion(bf16[2048,256]{1,0:T(8,128)(2,1)} %param.42, bf16[8,2048]{1,0:T(8,128)(2,1)S(1)} %get-tuple-element.118, f32[2048]{0:T(1024)S(1)} %convert_element_type.128, f32[8]{0:T(128)S(1)} %add_rsqrt_fusion.1), kind=kOutput, calls=%fused_computation.118 | convolution fusion | flops 8454144 | bytes 1097760 | tf_op jit(solution)/shard_map/dot_general | solution.py:37
  92.6 20.7 %all-to-all-done.2 = bf16[16,12,2048]{2,1,0:T(8,128)(2,1)S(1)} async-done(((bf16[16,12,2048]{2,1,0:T(8,128)(2,1)}), bf16[16,12,2048]{2,1,0:T(8,128)(2,1)S(1)}, u32[]{:S(2)}, u32[]{:S(2)}) %all-to-all-start.2) | async-done | bytes 786464 | tf_op jit(solution)/shard_map/all_to_all | solution.py:169
  113.4 0.7 gather_fusion
  114.4 2.4 %multiply_reduce_fusion.1 = (f32[8]{0:T(128)S(1)}, f32[8,2048]{1,0:T(8,128)S(1)}) fusion(f32[8,2048]{1,0:T(8,128)S(1)} %multiply_reduce_fusion, bf16[256,2048]{1,0:T(8,128)(2,1)} %param.44, bf16[2048,256]{1,0:T(8,128)(2,1)} %param.43, f32[8,256]{1,0:T(8,128)S(1)} %fusion.72, bf16[8,2048]{1,0:T(8,128)(2,1)S(1)} %get-tuple-element.118, ...), kind=kOutput, calls=%fused_computation.69 | convolution fusion | flops 16936952 | bytes 2277440 | tf_op jit(solution)/shard_map/dot_general | solution.py:40
  116.8 0.7 fusion.47
  (70 shorter events, 5.2 us)
Async XLA Ops:
  0.0 83.4 %copy-start = (bf16[1,256,2048]{2,1,0:T(8,128)(2,1)S(1)}, bf16[1,256,2048]{2,1,0:T(8,128)(2,1)}, u32[]{:S(2)}) copy-start(bf16[1,256,2048]{2,1,0:T(8,128)(2,1)} %param.41) | copy-start | bytes 3145732
  7.0 6.7 %copy-start.2 = (bf16[256,16,128]{2,1,0:T(8,128)(2,1)S(1)}, bf16[256,16,128]{2,1,0:T(8,128)(2,1)}, u32[]{:S(2)}) copy-start(bf16[256,16,128]{2,1,0:T(8,128)(2,1)} %param.33) | copy-start | bytes 3145732
  7.1 35.0 %copy-start.3 = (bf16[2048,128]{1,0:T(8,128)(2,1)S(1)}, bf16[2048,128]{1,0:T(8,128)(2,1)}, u32[]{:S(2)}) copy-start(bf16[2048,128]{1,0:T(8,128)(2,1)} %param.34) | copy-start | bytes 1572868
  7.1 39.4 %copy-start.5 = (bf16[2048]{0:T(1024)(128)(2,1)S(1)}, bf16[2048]{0:T(1024)(128)(2,1)}, u32[]{:S(2)}) copy-start(bf16[2048]{0:T(1024)(128)(2,1)} %param.35) | copy-start | bytes 12292
  7.1 39.5 %copy-start.6 = (s32[16,6]{0,1:T(8,128)S(1)}, s32[16,6]{0,1:T(8,128)}, u32[]{:S(2)}) copy-start(s32[16,6]{0,1:T(8,128)} %param.38) | copy-start | bytes 1156
  7.1 40.0 %copy-start.7 = (bf16[2048]{0:T(1024)(128)(2,1)S(1)}, bf16[2048]{0:T(1024)(128)(2,1)}, u32[]{:S(2)}) copy-start(bf16[2048]{0:T(1024)(128)(2,1)} %param.36) | copy-start | bytes 12292
  7.1 46.1 %copy-start.4 = (bf16[8,2048]{1,0:T(8,128)(2,1)S(1)}, bf16[8,2048]{1,0:T(8,128)(2,1)}, u32[]{:S(2)}) copy-start(bf16[8,2048]{1,0:T(8,128)(2,1)} %param.24) | copy-start | bytes 98308
  43.0 10.1 %all-to-all-start = ((bf16[16,8,128]{2,1,0:T(8,128)(2,1)}), bf16[16,8,128]{2,1,0:T(8,128)(2,1)S(1)}, u32[]{:S(2)}, u32[]{:S(2)}) async-start(bf16[16,8,128]{2,1,0:T(8,128)(2,1)} %fusion.23), calls=%async_computation | async-start | bytes 65536 | tf_op jit(solution)/shard_map/all_to_all | solution.py:125
  54.1 29.3 %copy-start.1 = (bf16[1,2048,256]{2,1,0:T(8,128)(2,1)S(1)}, bf16[1,2048,256]{2,1,0:T(8,128)(2,1)}, u32[]{:S(2)}) copy-start(bf16[1,2048,256]{2,1,0:T(8,128)(2,1)} %param.40) | copy-start | bytes 3145732
  81.8 8.7 %copy-start.8 = (bf16[2048]{0:T(1024)(128)(2,1)S(1)}, bf16[2048]{0:T(1024)(128)(2,1)}, u32[]{:S(2)}) copy-start(bf16[2048]{0:T(1024)(128)(2,1)} %param.45) | copy-start | bytes 12292
  81.8 8.7 %copy-start.9 = (bf16[2048,16]{0,1:T(8,128)(2,1)S(1)}, bf16[2048,16]{0,1:T(8,128)(2,1)}, u32[]{:S(2)}) copy-start(bf16[2048,16]{0,1:T(8,128)(2,1)} %param.37) | copy-start | bytes 196612
  85.4 27.8 %all-to-all-start.2 = ((bf16[16,12,2048]{2,1,0:T(8,128)(2,1)}), bf16[16,12,2048]{2,1,0:T(8,128)(2,1)S(1)}, u32[]{:S(2)}, u32[]{:S(2)}) async-start(bf16[16,12,2048]{2,1,0:T(8,128)(2,1)} %bitcast.17), calls=%async_computation.2 | async-start | bytes 2097152 | tf_op jit(solution)/shard_map/all_to_all | solution.py:169
where the time goes:
time: 120 us; the launch traced here: 118 us
  blocking collectives  55.4 us (46%)
  waiting for transfers between devices  26.6 us (22%)
  matrix products  15.1 us (13%)
  starting transfers between devices  8.43 us (7%)
  other arithmetic  7.86 us (7%)
  local copies, waits for them, and re-layouts  3.09 us (3%)
    all_gather x1, blocking collectives, local(): lax.all_gather(heads_out, ('ep', 'tp'), axis=0, tiled=True)  28 us
    all_to_all x1, blocking collectives, local(): lax.all_to_all(outgoing, ('ep', 'tp'), split_axis=0, concat_axis=0, tiled...  27.4 us
    all_to_all x1, waiting for transfers between devices, local(): lax.all_to_all(copies, ('ep', 'tp'), split_axis=0, concat_axis=0, tiled=T...  20.7 us
    all_to_all x1, waiting for transfers between devices, local(): lax.all_to_all(column_rows, ('ep', 'tp'), split_axis=0, concat_axis=1, ti...  5.92 us
    all_to_all x1, starting transfers between devices, local(): lax.all_to_all(copies, ('ep', 'tp'), split_axis=0, concat_axis=0, tiled=T...  4.94 us
    all_to_all x1, starting transfers between devices, local(): lax.all_to_all(column_rows, ('ep', 'tp'), split_axis=0, concat_axis=1, ti...  3.5 us
    dot_general x2, matrix products, swiglu(): jnp.dot(inner_rows, down_w, preferred_element_type=jnp.float32)  3.18 us
    dot_general x2, matrix products, swiglu(): gate_part = jnp.dot(flat_rows, gate_w, preferred_element_type=jnp.float32)  3.07 us
  transfers between devices with their start and end apart: 2, of which 2 were waited for; matrix products, arithmetic and copies ran while one was open for 2% of the time, Pallas kernels for 0%

commit v1 on v0

--- a/solution.py
+++ b/solution.py
@@ -1,6 +1,10 @@
+import functools
+
 import jax
 import jax.numpy as jnp
 from jax import lax
+from jax.experimental import pallas as pl
+from jax.experimental.pallas import tpu as pltpu
 from jax.sharding import PartitionSpec as P
 
 ABLK = 512
@@ -40,7 +44,7 @@
     return jnp.dot(inner_rows, down_w, preferred_element_type=jnp.float32).astype(jnp.bfloat16)
 
 
-def local(
+def local_wide(
     hidden_in,
     query_nope,
     query_rope,
@@ -176,6 +180,460 @@
     ).astype(jnp.bfloat16)
 
 
+def fused_kernel(
+    grid_p,
+    grid_q,
+    score_scale,
+    ql_ref,
+    qp_ref,
+    lnew_ref,
+    knew_ref,
+    len_ref,
+    own_ref,
+    cl_hbm,
+    cr_hbm,
+    vup_hbm,
+    wo_hbm,
+    gain_ref,
+    router_hbm,
+    eg_hbm,
+    eu_hbm,
+    ed_hbm,
+    sg_hbm,
+    su_hbm,
+    sd_hbm,
+    out_ref,
+    cl,
+    cr,
+    vup,
+    wo,
+    router,
+    eg,
+    eu,
+    ed,
+    sg,
+    su,
+    sd,
+    xbuf,
+    hbuf,
+    cbuf,
+    lat,
+    norm_rows,
+    mix_rows,
+    terms,
+    sib,
+    part,
+    back,
+    cache_sem,
+    rope_sem,
+    weight_sem,
+    ag_send,
+    ag_recv,
+    sib_send,
+    sib_recv,
+    back_send,
+    back_recv,
+):
+    seq_count, heads, latent = ql_ref.shape
+    width = out_ref.shape[1]
+    ep_count = grid_p * grid_q
+    device_count = 2 * ep_count
+    total_rows = device_count * seq_count
+    me_e = lax.axis_index("ep")
+    me_t = lax.axis_index("tp")
+    other_t = 1 - me_t
+    p = me_e // grid_q
+    q = me_e % grid_q
+    me = me_e * 2 + me_t
+
+    def device(e, t):
+        return {"ep": e, "tp": t}
+
+    sibling = device(me_e, other_t)
+    barrier = pltpu.get_barrier_semaphore()
+    for step in range(1, ep_count):
+        pl.semaphore_signal(
+            barrier,
+            inc=1,
+            device_id=device((me_e + step) % ep_count, me_t),
+            device_id_type=pl.DeviceIdType.MESH,
+        )
+    pl.semaphore_signal(
+        barrier, inc=1, device_id=sibling, device_id_type=pl.DeviceIdType.MESH
+    )
+
+    cache_copies = []
+    for s in range(seq_count):
+        pair = (
+            pltpu.make_async_copy(cl_hbm.at[s], cl.at[s], cache_sem.at[s]),
+            pltpu.make_async_copy(cr_hbm.at[s], cr.at[s], rope_sem.at[s]),
+        )
+        pair[0].start()
+        pair[1].start()
+        cache_copies.append(pair)
+    weight_copies = []
+    moves = (
+        (vup_hbm, vup),
+        (wo_hbm, wo),
+        (router_hbm, router),
+        (eg_hbm, eg),
+        (eu_hbm, eu),
+        (ed_hbm, ed),
+        (sg_hbm, sg),
+        (su_hbm, su),
+        (sd_hbm, sd),
+    )
+    for index, (source, target) in enumerate(moves):
+        copy = pltpu.make_async_copy(source, target, weight_sem.at[index])
+        copy.start()
+        weight_copies.append(copy)
+    xbuf[me] = own_ref[...]
+
+    line_steps = list(range(1, grid_p))
+    pending = []
+
+    class Gather:
+        def __init__(self, buf, which):
+            self.buf, self.which, self.count = buf, which, 0
+
+        def send(self, slot, target):
+            copy = pltpu.make_async_remote_copy(
+                src_ref=self.buf.at[slot],
+                dst_ref=self.buf.at[slot],
+                send_sem=ag_send.at[self.which, self.count],
+                recv_sem=ag_recv.at[self.which, slot],
+                device_id=target,
+                device_id_type=pl.DeviceIdType.MESH,
+            )
+            copy.start()
+            pending.append(copy)
+            self.count += 1
+
+        def arrive(self, slot):
+            pltpu.make_async_remote_copy(
+                src_ref=self.buf.at[slot],
+                dst_ref=self.buf.at[slot],
+                send_sem=ag_send.at[self.which, 0],
+                recv_sem=ag_recv.at[self.which, slot],
+                device_id=sibling,
+                device_id_type=pl.DeviceIdType.MESH,
+            ).wait_recv()
+
+        def line(self, step):
+            return (p + step) % grid_p
+
+        def first(self):
+            for step in sorted(line_steps, key=lambda v: -min(v, grid_p - v)):
+                self.send(me, device(self.line(step) * grid_q + q, me_t))
+            for turn in range(1, grid_q):
+                self.send(me, device(p * grid_q + (q + turn) % grid_q, me_t))
+            self.send(me, sibling)
+
+        def second(self):
+            for step in sorted(line_steps, key=lambda v: min(v, grid_p - v)):
+                slot = (self.line(step) * grid_q + q) * 2 + me_t
+                self.arrive(slot)
+                for turn in range(1, grid_q):
+                    self.send(slot, device(p * grid_q + (q + turn) % grid_q, me_t))
+                self.send(slot, sibling)
+
+        def third(self):
+            for step in sorted([0] + line_steps, key=lambda v: min(v, grid_p - v)):
+                for turn in range(1, grid_q):
+                    slot = (self.line(step) * grid_q + (q + turn) % grid_q) * 2 + me_t
+                    self.arrive(slot)
+                    self.send(slot, sibling)
+
+        def last(self):
+            for e in range(ep_count):
+                self.arrive(e * 2 + other_t)
+
+    context = cl.shape[1]
+    key_index = lax.broadcasted_iota(jnp.int32, (heads, context), 1)
+
+    def attend(s):
+        cache_copies[s][0].wait()
+        cache_copies[s][1].wait()
+        q_lat = ql_ref[s]
+        q_pe = qp_ref[s]
+        keys = cl[s]
+        dims = (((1,), (1,)), ((), ()))
+        scores = (
+            lax.dot_general(q_lat, keys, dims, preferred_element_type=jnp.float32)
+            + lax.dot_general(q_pe, cr[s], dims, preferred_element_type=jnp.float32)
+        ) * score_scale
+        new_row = lnew_ref[s : s + 1, :].astype(jnp.float32)
+        key_row = knew_ref[s : s + 1, :].astype(jnp.float32)
+        new_score = (
+            jnp.sum(q_lat.astype(jnp.float32) * new_row, axis=-1, keepdims=True)
+            + jnp.sum(q_pe.astype(jnp.float32) * key_row, axis=-1, keepdims=True)
+        ) * score_scale
+        scores = jnp.where(key_index < len_ref[s], scores, masked_score)
+        row_max = jnp.maximum(jnp.max(scores, axis=-1, keepdims=True), new_score)
+        weights = jnp.exp(scores - row_max)
+        new_weight = jnp.exp(new_score - row_max)
+        weight_total = jnp.sum(weights, axis=-1, keepdims=True) + new_weight
+        weighted = jnp.dot(weights.astype(jnp.bfloat16), keys, preferred_element_type=jnp.float32)
+        weighted = weighted + new_weight.astype(jnp.bfloat16).astype(jnp.float32) * new_row
+        lat[s * heads : (s + 1) * heads, :] = (weighted / weight_total).astype(jnp.bfloat16)
+
+    rows_gather = Gather(xbuf, 0)
+    cut_a, cut_b = seq_count // 2, seq_count - seq_count // 4
+    for s in range(cut_a):
+        attend(s)
+    pl.semaphore_wait(barrier, ep_count)
+    rows_gather.first()
+    for s in range(cut_a, cut_b):
+        attend(s)
+    rows_gather.second()
+    for s in range(cut_b, seq_count):
+        attend(s)
+
+    weight_copies[0].wait()
+    value_dim = width_of_head(vup, heads)
+    spread = jnp.dot(lat[...], vup[...], preferred_element_type=jnp.float32)
+    own_heads = []
+    head_row = lax.broadcasted_iota(jnp.int32, (seq_count, heads, value_dim), 1)
+    for h in range(heads):
+        block = spread[:, h * value_dim : (h + 1) * value_dim].reshape(seq_count, heads, value_dim)
+        own_heads.append(jnp.sum(jnp.where(head_row == h, block, 0.0), axis=1))
+    hbuf[me] = jnp.concatenate(own_heads, axis=1).astype(jnp.bfloat16)
+    heads_gather = Gather(hbuf, 1)
+    heads_gather.first()
+    rows_gather.third()
+    heads_gather.second()
+    heads_gather.third()
+    rows_gather.last()
+    weight_copies[1].wait()
+    heads_gather.last()
+
+    flat_heads = hbuf[...].reshape(total_rows, hbuf.shape[2])
+    cbuf[me] = jnp.dot(flat_heads, wo[...], preferred_element_type=jnp.float32).astype(jnp.bfloat16)
+    columns_gather = Gather(cbuf, 2)
+    columns_gather.first()
+    columns_gather.second()
+    columns_gather.third()
+    columns_gather.last()
+
+    gains = gain_ref[...].astype(jnp.float32)
+    mixed = jnp.concatenate([cbuf[o] for o in range(device_count)], axis=1).astype(jnp.float32)
+    stage = xbuf[...].reshape(total_rows, xbuf.shape[2])
+    after_mix = (stage[:, :width].astype(jnp.float32) + gains[0:1] * normalize(mixed)).astype(
+        jnp.bfloat16
+    )
+    mix_rows[...] = after_mix.reshape(mix_rows.shape)
+    ffn_in = (normalize(after_mix.astype(jnp.float32)) * gains[1:2]).astype(jnp.bfloat16)
+    norm_rows[...] = ffn_in.reshape(norm_rows.shape)
+    weight_copies[2].wait()
+    affinity = jax.nn.sigmoid(jnp.dot(ffn_in, router[...], preferred_element_type=jnp.float32))
+    hot = stage[:, width : width + affinity.shape[1]].astype(jnp.float32)
+    chosen = affinity * hot
+    lane = lax.broadcasted_iota(jnp.int32, chosen.shape, 1)
+    mine = jnp.sum(jnp.where(lane == me, chosen, 0.0), axis=1, keepdims=True)
+    mine = mine / jnp.sum(chosen, axis=1, keepdims=True) * routed_scale
+    for copy in weight_copies[3:6]:
+        copy.wait()
+    expert_out = swiglu(ffn_in, eg[...], eu[...], ed[...])
+    scaled = (expert_out.astype(jnp.float32) * mine).astype(jnp.bfloat16)
+    terms[...] = scaled.reshape(terms.shape)
+
+    def to_sibling(step):
+        e = (me_e + step) % ep_count
+        return pltpu.make_async_remote_copy(
+            src_ref=terms.at[e * 2 + other_t],
+            dst_ref=sib.at[e],
+            send_sem=sib_send.at[step],
+            recv_sem=sib_recv.at[e],
+            device_id=sibling,
+            device_id_type=pl.DeviceIdType.MESH,
+        )
+
+    order = sorted(range(1, ep_count), key=lambda v: -min(v, ep_count - v)) + [0]
+    sib_copies = [to_sibling(step) for step in order]
+    for copy in sib_copies:
+        copy.start()
+    sends = []
+    for step in order:
+        e = (me_e + step) % ep_count
+        to_sibling(step).wait_recv()
+        paired = terms[e * 2 + me_t].astype(jnp.float32) + sib[e].astype(jnp.float32)
+        if step == 0:
+            routed = paired
+        else:
+            part[e] = paired.astype(jnp.bfloat16)
+            copy = pltpu.make_async_remote_copy(
+                src_ref=part.at[e],
+                dst_ref=back.at[me_e],
+                send_sem=back_send.at[step],
+                recv_sem=back_recv.at[me_e],
+                device_id=device(e, me_t),
+                device_id_type=pl.DeviceIdType.MESH,
+            )
+            copy.start()
+            sends.append(copy)
+    for copy in weight_copies[6:9]:
+        copy.wait()
+    combined = routed + swiglu(norm_rows[me], sg[...], su[...], sd[...]).astype(jnp.float32)
+    for step in reversed(order[:-1]):
+        e = (me_e + step) % ep_count
+        pltpu.make_async_remote_copy(
+            src_ref=part.at[e],
+            dst_ref=back.at[e],
+            send_sem=back_send.at[step],
+            recv_sem=back_recv.at[e],
+            device_id=device(e, me_t),
+            device_id_type=pl.DeviceIdType.MESH,
+        ).wait_recv()
+        combined = combined + back[e].astype(jnp.float32)
+    out_ref[...] = (
+        mix_rows[me].astype(jnp.float32) + gains[2:3] * normalize(combined)
+    ).astype(jnp.bfloat16)
+    for copy in pending + sib_copies + sends:
+        copy.wait_send()
+
+
+def width_of_head(flat, heads):
+    return flat.shape[1] // heads
+
+
+def local_fused(
+    hidden_in,
+    query_nope,
+    query_rope,
+    new_latent,
+    new_rope,
+    cache_latent,
+    cache_rope,
+    lengths,
+    absorb_key,
+    value_up,
+    out_proj,
+    gain_mix,
+    gain_ffn_in,
+    router,
+    routes,
+    expert_gate,
+    expert_up,
+    expert_down,
+    shared_gate,
+    shared_up,
+    shared_down,
+    gain_ffn_out,
+):
+    seq_count, width = hidden_in.shape
+    heads, latent = query_nope.shape[1], cache_latent.shape[2]
+    ep_count = lax.axis_size("ep")
+    device_count = 2 * ep_count
+    bits = (ep_count - 1).bit_length()
+    grid_p = 2 ** ((bits + 1) // 2)
+    grid_q = ep_count // grid_p
+    positions = lengths.astype(jnp.float32)
+    query_latent = jnp.einsum(
+        "shn,chn->shc", query_nope, absorb_key, preferred_element_type=jnp.float32
+    ).astype(jnp.bfloat16)
+    query_pe = rotate(query_rope.astype(jnp.float32), positions[:, None, None]).astype(jnp.bfloat16)
+    latent_new = normalize(new_latent.astype(jnp.float32)).astype(jnp.bfloat16)
+    key_new = rotate(new_rope.astype(jnp.float32), positions[:, None]).astype(jnp.bfloat16)
+    own_start = lax.axis_index("tp") * seq_count
+    own_routes = lax.dynamic_slice_in_dim(routes, own_start, seq_count, 0)
+    hot = jnp.any(
+        own_routes[:, :, None] == lax.iota(jnp.int32, 128)[None, None, :], axis=1
+    ).astype(jnp.bfloat16)
+    own = jnp.concatenate([hidden_in, hot], axis=1)
+    gains = jnp.stack([gain_mix, gain_ffn_in, gain_ffn_out])
+    value_flat = value_up.reshape(value_up.shape[0], -1)
+    bf = jnp.bfloat16
+    score_scale = (query_nope.shape[-1] + query_rope.shape[-1]) ** (-0.5)
+    sends = (grid_p - 1) + grid_p * (grid_q - 1) + ep_count
+    big = pl.BlockSpec(memory_space=pl.ANY)
+    near = pl.BlockSpec(memory_space=pltpu.VMEM)
+    dma = pltpu.SemaphoreType.DMA
+    total_rows = device_count * seq_count
+    weights = (
+        value_flat,
+        out_proj,
+        router,
+        expert_gate[0],
+        expert_up[0],
+        expert_down[0],
+        shared_gate,
+        shared_up,
+        shared_down,
+    )
+    operands = (
+        query_latent,
+        query_pe,
+        latent_new,
+        key_new,
+        lengths,
+        own,
+        cache_latent,
+        cache_rope,
+        value_flat,
+        out_proj,
+        gains,
+        router,
+    ) + weights[3:]
+    specs = (
+        [near] * 4
+        + [pl.BlockSpec(memory_space=pltpu.SMEM), near]
+        + [big] * 4
+        + [near]
+        + [big] * 7
+    )
+    flops = 2 * total_rows * width * out_proj.shape[1]
+    return pl.pallas_call(
+        functools.partial(fused_kernel, grid_p, grid_q, score_scale),
+        out_shape=jax.ShapeDtypeStruct((seq_count, width), bf),
+        in_specs=specs,
+        out_specs=near,
+        scratch_shapes=[
+            pltpu.VMEM(cache_latent.shape, bf),
+            pltpu.VMEM(cache_rope.shape, bf),
+        ]
+        + [pltpu.VMEM(w.shape, bf) for w in weights]
+        + [
+            pltpu.VMEM((device_count,) + own.shape, bf),
+            pltpu.VMEM((device_count, seq_count, out_proj.shape[0]), bf),
+            pltpu.VMEM((device_count, total_rows, out_proj.shape[1]), bf),
+            pltpu.VMEM((seq_count * heads, latent), bf),
+            pltpu.VMEM((device_count, seq_count, width), bf),
+            pltpu.VMEM((device_count, seq_count, width), bf),
+            pltpu.VMEM((device_count, seq_count, width), bf),
+            pltpu.VMEM((ep_count, seq_count, width), bf),
+            pltpu.VMEM((ep_count, seq_count, width), bf),
+            pltpu.VMEM((ep_count, seq_count, width), bf),
+            dma((seq_count,)),
+            dma((seq_count,)),
+            dma((len(weights),)),
+            dma((3, sends)),
+            dma((3, device_count)),
+            dma((ep_count,)),
+            dma((ep_count,)),
+            dma((ep_count,)),
+            dma((ep_count,)),
+        ],
+        compiler_params=pltpu.CompilerParams(
+            collective_id=0, has_side_effects=True, vmem_limit_bytes=56 * 2**20
+        ),
+        cost_estimate=pl.CostEstimate(flops=flops, bytes_accessed=2**24, transcendentals=0),
+        name="layer_step",
+    )(*operands)
+
+
+def local(*args):
+    hidden_in, out_proj, router = args[0], args[10], args[13]
+    device_count = lax.axis_size("ep") * lax.axis_size("tp")
+    fits = (
+        lax.axis_size("tp") == 2
+        and hidden_in.shape[0] == 8
+        and device_count * hidden_in.shape[0] <= 256
+        and out_proj.shape[1] % 128 == 0
+        and router.shape[1] == device_count
+    )
+    return local_fused(*args) if fits else local_wide(*args)
+
+
 def solution(mesh):
     placed = (
         P(("grp", "ep", "tp"), None),

time: 120 us -> 65.8 us (0.55); the launches traced: 118 us -> 65 us
  blocking collectives: 55.4 us -> 0 us
  Pallas kernels: 0 us -> 45.1 us
  waiting for transfers between devices: 26.6 us -> 0 us
  matrix products: 15.1 us -> 0.92 us
  starting transfers between devices: 8.43 us -> 0 us
  local copies, waits for them, and re-layouts: 3.09 us -> 11 us
    pallas_call x0 -> x1, Pallas kernels: none -> 45.1 us  [local_fused(): pl.pallas_call(functools.partial(fused_kernel, grid_p, grid_q, score_scal...]
    all_gather x1 -> x0, blocking collectives: 28 us -> none  [local(): lax.all_gather(heads_out, ('ep', 'tp'), axis=0, tiled=True)]
    all_to_all x1 -> x0, blocking collectives: 27.4 us -> none  [local(): lax.all_to_all(outgoing, ('ep', 'tp'), split_axis=0, concat_axis=0, tiled...]
    all_to_all x2 -> x0, waiting for transfers between devices: 26.6 us -> none  [the longest x1 20.7 us: local(): lax.all_to_all(copies, ('ep', 'tp'), split_axis=0, concat_axis=0, tiled=T...]
    dot_general x14 -> x1, matrix products: 15.1 us -> 0.92 us  [local_fused(): jnp.einsum('shn,chn->shc', query_nope, absorb_key, preferred_element_type...]
    all_to_all x2 -> x0, starting transfers between devices: 8.43 us -> none  [the longest x1 4.94 us: local(): lax.all_to_all(copies, ('ep', 'tp'), split_axis=0, concat_axis=0, tiled=T...]
    unnamed x21 -> x8, local copies, waits for them, and re-layouts: 0.14 us -> 7.48 us
    another operation x1 -> x3, local copies, waits for them, and re-layouts: 0.01 us -> 2.08 us  [local_fused(): gains = jnp.stack([gain_mix, gain_ffn_in, gain_ffn_out])]
  transfers between devices with their start and end apart: 2 -> 0, of which waited for: 2 -> 0; matrix products, arithmetic and copies ran while one was open for 2% -> 0% of each run, Pallas kernels for 0% -> 0%
where the time goes in v1:
time: 65.8 us; the launch traced here: 65 us
  Pallas kernels  45.1 us (69%)
  local copies, waits for them, and re-layouts  11 us (17%)
  other arithmetic  8.02 us (12%)
  matrix products  0.92 us (1%)
    pallas_call x1, Pallas kernels, local_fused(): pl.pallas_call(functools.partial(fused_kernel, grid_p, grid_q, score_scal...  45.1 us
    unnamed x8, local copies, waits for them, and re-layouts  7.48 us
    another operation x3, local copies, waits for them, and re-layouts, local_fused(): gains = jnp.stack([gain_mix, gain_ffn_in, gain_ffn_out])  2.08 us
    concatenate x2, other arithmetic, rotate(): jnp.concatenate([first_half * cosine - second_half * sine_table, first_ha...  1.37 us
    concatenate x1, other arithmetic, local_fused(): own = jnp.concatenate([hidden_in, hot], axis=1)  1.36 us
    convert_element_type x1, other arithmetic, local_fused(): latent_new = normalize(new_latent.astype(jnp.float32)).astype(jnp.bfloat16)  1.35 us

profile of v1, /device:TPU:0, one launch (start us, length us, event | category | flops | bytes accessed | tf_op | source)
XLA Modules:
  0.0 65.0 jit_solution(11857906117085195324)
XLA Ops:
  0.0 0.0 copy-start
  0.0 0.9 %fusion.4 = f32[8]{0:T(128)S(1)} fusion(bf16[8,256]{1,0:T(8,128)(2,1)} %param.25), kind=kLoop, calls=%fused_computation.14 | loop fusion | flops 6136 | bytes 4128 | tf_op jit(solution)/shard_map/reduce_sum | solution.py:20
  0.9 0.7 %convert_element_type.28 = f32[8]{0:T(128)S(1)} convert(s32[8]{0:T(128)} %len_ref.1) | non-fusion elementwise | flops 8 | bytes 64 | tf_op jit(solution)/shard_map/convert_element_type | solution.py:530
  1.6 1.4 %fusion.5.lnew_ref = bf16[8,256]{1,0:T(8,128)(2,1)} fusion(bf16[8,256]{1,0:T(8,128)(2,1)} %param.25, f32[8]{0:T(128)S(1)} %add_rsqrt_fusion), kind=kLoop, calls=%fused_computation.15 | loop fusion | flops 6144 | bytes 8224 | tf_op jit(solution)/shard_map/convert_element_type | solution.py:535
  2.9 0.8 %constant_dynamic-slice_fusion = s32[8,6]{0,1:T(8,128)S(1)} fusion(s32[16,6]{0,1:T(8,128)} %param.36, s32[]{:T(128)S(6)} %select_n.3), kind=kLoop, calls=%fused_computation.23 | loop fusion | bytes 388 | tf_op jit(solution)/shard_map/dynamic_slice | solution.py:538
  3.7 0.1 fusion.3
  3.8 0.7 %convert_element_type.31 = f32[8,32]{1,0:T(8,128)S(1)} convert(bf16[8,32]{1,0:T(8,128)(2,1)} %param.26) | non-fusion elementwise | flops 256 | bytes 1536 | tf_op jit(solution)/shard_map/convert_element_type | solution.py:536
  4.5 0.1 subtract_convert_fusion.1
  4.6 0.7 %pad_maximum_fusion.3.knew_ref = bf16[8,32]{1,0:T(8,128)(2,1)} fusion(bf16[8,16]{1,0:T(8,128)(2,1)S(1)} %get-tuple-element.8, bf16[8,16]{1,0:T(8,128)(2,1)S(1)} %get-tuple-element.7), kind=kLoop, calls=%fused_computation.20 | loop fusion | flops 1024 | bytes 1024 | tf_op jit(solution)/shard_map/concatenate | solution.py:31
  5.2 0.7 %stack.12 = bf16[1,2048]{1,0:T(2,128)(2,1)S(1)} reshape(bf16[2048]{0:T(1024)(128)(2,1)} %param.33) | data formatting | bytes 8192 | tf_op jit(solution)/shard_map/stack | solution.py:543
  5.9 0.7 %stack.13 = bf16[1,2048]{1,0:T(2,128)(2,1)S(1)} reshape(bf16[2048]{0:T(1024)(128)(2,1)} %param.34) | data formatting | bytes 8192 | tf_op jit(solution)/shard_map/stack | solution.py:543
  6.6 0.7 %stack.14 = bf16[1,2048]{1,0:T(2,128)(2,1)S(1)} reshape(bf16[2048]{0:T(1024)(128)(2,1)} %param.43) | data formatting | bytes 8192 | tf_op jit(solution)/shard_map/stack | solution.py:543
  7.3 0.6 pad_maximum_fusion.2.gain_ref
  8.0 1.4 %pad_maximum_fusion.own_ref = bf16[8,2176]{1,0:T(8,128)(2,1)} fusion(bf16[8,128]{1,0:T(8,128)(2,1)S(1)} %convert_element_type.32, bf16[8,2048]{1,0:T(8,128)(2,1)} %param.22), kind=kLoop, calls=%fused_computation.5 | loop fusion | flops 69632 | bytes 69632 | tf_op jit(solution)/shard_map/concatenate | solution.py:542
  9.3 0.9 %fusion.1 = bf16[16,256,8]{1,2,0:T(8,128)(2,1)S(1)} fusion(bf16[256,16,64]{0,2,1:T(8,128)(2,1)S(1)} %copy-done, bf16[8,16,64]{2,1,0:T(8,128)(2,1)} %param.23), kind=kOutput, calls=%fused_computation.7 | convolution fusion | flops 4194304 | bytes 606208 | tf_op jit(solution)/shard_map/shn,chn->shc/dot_general | solution.py:531
  10.2 0.6 copy.40
  10.9 0.8 %convert_element_type.27 = f32[8,16,32]{2,1,0:T(8,128)S(1)} convert(bf16[8,16,32]{2,1,0:T(8,128)(2,1)} %param.24) | non-fusion elementwise | flops 4096 | bytes 24576 | tf_op jit(solution)/shard_map/convert_element_type | solution.py:534
  11.7 0.1 subtract_convert_fusion
  11.8 0.7 %pad_maximum_fusion.1.qp_ref = bf16[8,16,32]{2,1,0:T(8,128)(2,1)} fusion(bf16[8,16,16]{2,1,0:T(8,128)(2,1)S(1)} %get-tuple-element.6, bf16[8,16,16]{2,1,0:T(8,128)(2,1)S(1)} %get-tuple-element.5), kind=kLoop, calls=%fused_computation.6 | loop fusion | flops 16384 | bytes 16384 | tf_op jit(solution)/shard_map/concatenate | solution.py:31
  12.5 1.8 %copy.31.router_hbm = bf16[2048,16]{1,0:T(8,128)(2,1)} copy(bf16[2048,16]{0,1:T(8,128)(2,1)} %param.35) | data formatting | bytes 131072 | tf_op args[13]
  14.3 2.5 %copy.39 = bf16[32,8,16,128]{3,1,2,0:T(8,128)(2,1)} copy(bf16[32,8,16,128]{3,2,1,0:T(8,128)(2,1)} %bitcast.15) | data formatting | bytes 2097152
  16.8 1.8 %copy.30.cr_hbm = bf16[8,1024,32]{2,1,0:T(8,128)(2,1)} copy(bf16[8,1024,32]{1,2,0:T(8,128)(2,1)S(1)} %copy-done.1) | data formatting | bytes 1048576 | tf_op args[6]
  18.6 45.1 %layer_step.1 = bf16[8,2048]{1,0:T(8,128)(2,1)} custom-call(bf16[8,16,256]{2,1,0:T(8,128)(2,1)} %bitcast.16, bf16[8,16,32]{2,1,0:T(8,128)(2,1)} %pad_maximum_fusion.1.qp_ref, bf16[8,256]{1,0:T(8,128)(2,1)} %fusion.5.lnew_ref, bf16[8,32]{1,0:T(8,128)(2,1)} %pad_maximum_fusion.3.knew_ref, s32[8]{0:T(128)} %len_ref.1, bf16[8,2176]{1,0:T(8,128)(2,1)} %pad_maximum_fusion.own_ref, ...), custom_call_target="tpu_custom_call" | custom-call | flops 67108864 | bytes 16777216 | tf_op jit(solution)/shard_map/layer_step/pallas_call | solution.py:585
  63.7 1.4 %copy.42 = bf16[8,2048]{1,0:T(8,128)(2,1)} copy(bf16[8,2048]{1,0:T(8,128)(2,1)} %layer_step.1) | data formatting | bytes 65536
  (6 shorter events, 0.0 us)
Async XLA Ops:
  0.0 9.3 %copy-start = (bf16[256,16,64]{0,2,1:T(8,128)(2,1)S(1)}, bf16[256,16,64]{0,2,1:T(8,128)(2,1)}, u32[]{:S(2)}) copy-start(bf16[256,16,64]{0,2,1:T(8,128)(2,1)} %param.30) | copy-start | bytes 1572868
  0.0 16.8 %copy-start.1 = (bf16[8,1024,32]{1,2,0:T(8,128)(2,1)S(1)}, bf16[8,1024,32]{1,2,0:T(8,128)(2,1)}, u32[]{:S(2)}) copy-start(bf16[8,1024,32]{1,2,0:T(8,128)(2,1)} %param.28) | copy-start | bytes 1572868

commit v2 on v1

--- a/solution.py
+++ b/solution.py
@@ -184,17 +184,21 @@
     grid_p,
     grid_q,
     score_scale,
-    ql_ref,
-    qp_ref,
-    lnew_ref,
-    knew_ref,
+    hidden_ref,
+    qn_ref,
+    qr_ref,
+    nl_ref,
+    nr_ref,
     len_ref,
-    own_ref,
+    routes_ref,
+    gm_ref,
+    gf_ref,
+    go_ref,
+    ab_hbm,
     cl_hbm,
     cr_hbm,
     vup_hbm,
     wo_hbm,
-    gain_ref,
     router_hbm,
     eg_hbm,
     eu_hbm,
@@ -206,6 +210,11 @@
     cl,
     cr,
     vup,
+    wide_up,
+    ql_ref,
+    qp_ref,
+    ab,
+    vraw,
     wo,
     router,
     eg,
@@ -234,7 +243,8 @@
     back_send,
     back_recv,
 ):
-    seq_count, heads, latent = ql_ref.shape
+    seq_count, heads, nope = qn_ref.shape
+    rope = qr_ref.shape[2]
     width = out_ref.shape[1]
     ep_count = grid_p * grid_q
     device_count = 2 * ep_count
@@ -262,6 +272,11 @@
         barrier, inc=1, device_id=sibling, device_id_type=pl.DeviceIdType.MESH
     )
 
+    early_copies = []
+    for index, (source, target) in enumerate(((ab_hbm, ab), (vup_hbm, vraw))):
+        copy = pltpu.make_async_copy(source, target, weight_sem.at[index])
+        copy.start()
+        early_copies.append(copy)
     cache_copies = []
     for s in range(seq_count):
         pair = (
@@ -273,7 +288,6 @@
         cache_copies.append(pair)
     weight_copies = []
     moves = (
-        (vup_hbm, vup),
         (wo_hbm, wo),
         (router_hbm, router),
         (eg_hbm, eg),
@@ -284,10 +298,64 @@
         (sd_hbm, sd),
     )
     for index, (source, target) in enumerate(moves):
-        copy = pltpu.make_async_copy(source, target, weight_sem.at[index])
+        copy = pltpu.make_async_copy(source, target, weight_sem.at[index + 2])
         copy.start()
         weight_copies.append(copy)
-    xbuf[me] = own_ref[...]
+
+    xbuf[me, :, 0:width] = hidden_ref[...]
+    mark_shape = (seq_count, xbuf.shape[2] - width)
+    mark_row = lax.broadcasted_iota(jnp.int32, mark_shape, 0)
+    mark_lane = lax.broadcasted_iota(jnp.int32, mark_shape, 1)
+    marks = jnp.zeros(mark_shape, jnp.float32)
+    for s in range(seq_count):
+        for j in range(routes_ref.shape[0]):
+            expert = routes_ref[j, me_t * seq_count + s]
+            marks = jnp.where((mark_row == s) & (mark_lane == expert), 1.0, marks)
+    xbuf[me, :, width:] = marks.astype(jnp.bfloat16)
+
+    half = rope // 2
+    turn_row = lax.broadcasted_iota(jnp.int32, (seq_count, rope), 0)
+    turn_lane = lax.broadcasted_iota(jnp.int32, (seq_count, rope), 1)
+    position = jnp.zeros((seq_count, rope), jnp.float32)
+    for s in range(seq_count):
+        position = jnp.where(turn_row == s, len_ref[s].astype(jnp.float32), position)
+    inverse = jnp.zeros((seq_count, rope), jnp.float32)
+    for i in range(half):
+        inverse = jnp.where(turn_lane % half == i, rope_theta ** (-2.0 * i / rope), inverse)
+    angles = position * inverse
+    cosine = jnp.cos(angles)
+    sine = jnp.sin(angles) * jnp.where(turn_lane < half, -1.0, 1.0)
+
+    def turned(values, cos_rows, sin_rows):
+        swapped = jnp.concatenate([values[:, half:], values[:, :half]], axis=1)
+        return values * cos_rows + swapped * sin_rows
+
+    def per_head(table):
+        return jnp.broadcast_to(table[:, None, :], (seq_count, heads, rope)).reshape(
+            seq_count * heads, rope
+        )
+
+    query_rows = qr_ref[...].astype(jnp.float32).reshape(seq_count * heads, rope)
+    qp_ref[...] = turned(query_rows, per_head(cosine), per_head(sine)).astype(jnp.bfloat16)
+    key_rows = turned(nr_ref[...].astype(jnp.float32), cosine, sine).astype(jnp.bfloat16)
+    key_rows = key_rows.astype(jnp.float32)
+    new_rows = normalize(nl_ref[...].astype(jnp.float32)).astype(jnp.bfloat16).astype(jnp.float32)
+
+    nope_rows = qn_ref[...].astype(jnp.float32).reshape(seq_count * heads, nope)
+    row_head = lax.broadcasted_iota(jnp.int32, (seq_count * heads, 2 * nope), 0) % heads
+    pair_lane = lax.broadcasted_iota(jnp.int32, (seq_count * heads, 2 * nope), 1) // nope
+    doubled = jnp.concatenate([nope_rows, nope_rows], axis=1)
+    spread_query = jnp.concatenate(
+        [
+            jnp.where(row_head == pair_lane + 2 * j, doubled, 0.0).astype(jnp.bfloat16)
+            for j in range(heads // 2)
+        ],
+        axis=1,
+    )
+    early_copies[0].wait()
+    ql_ref[...] = jnp.dot(spread_query, ab[...], preferred_element_type=jnp.float32).astype(
+        jnp.bfloat16
+    )
 
     line_steps = list(range(1, grid_p))
     pending = []
@@ -354,16 +422,16 @@
     def attend(s):
         cache_copies[s][0].wait()
         cache_copies[s][1].wait()
-        q_lat = ql_ref[s]
-        q_pe = qp_ref[s]
+        q_lat = ql_ref[s * heads : (s + 1) * heads, :]
+        q_pe = qp_ref[s * heads : (s + 1) * heads, :]
         keys = cl[s]
         dims = (((1,), (1,)), ((), ()))
         scores = (
             lax.dot_general(q_lat, keys, dims, preferred_element_type=jnp.float32)
-            + lax.dot_general(q_pe, cr[s], dims, preferred_element_type=jnp.float32)
+            + jnp.dot(q_pe, cr[s], preferred_element_type=jnp.float32)
         ) * score_scale
-        new_row = lnew_ref[s : s + 1, :].astype(jnp.float32)
-        key_row = knew_ref[s : s + 1, :].astype(jnp.float32)
+        new_row = new_rows[s : s + 1, :]
+        key_row = key_rows[s : s + 1, :]
         new_score = (
             jnp.sum(q_lat.astype(jnp.float32) * new_row, axis=-1, keepdims=True)
             + jnp.sum(q_pe.astype(jnp.float32) * key_row, axis=-1, keepdims=True)
@@ -381,6 +449,11 @@
     cut_a, cut_b = seq_count // 2, seq_count - seq_count // 4
     for s in range(cut_a):
         attend(s)
+    early_copies[1].wait()
+    value_dim = vraw.shape[2]
+    wide_up[...] = vraw[...].astype(jnp.float32)
+    for h in range(heads):
+        vup[:, h * value_dim : (h + 1) * value_dim] = wide_up[:, h, :].astype(jnp.bfloat16)
     pl.semaphore_wait(barrier, ep_count)
     rows_gather.first()
     for s in range(cut_a, cut_b):
@@ -389,8 +462,6 @@
     for s in range(cut_b, seq_count):
         attend(s)
 
-    weight_copies[0].wait()
-    value_dim = width_of_head(vup, heads)
     spread = jnp.dot(lat[...], vup[...], preferred_element_type=jnp.float32)
     own_heads = []
     head_row = lax.broadcasted_iota(jnp.int32, (seq_count, heads, value_dim), 1)
@@ -404,7 +475,7 @@
     heads_gather.second()
     heads_gather.third()
     rows_gather.last()
-    weight_copies[1].wait()
+    weight_copies[0].wait()
     heads_gather.last()
 
     flat_heads = hbuf[...].reshape(total_rows, hbuf.shape[2])
@@ -415,23 +486,29 @@
     columns_gather.third()
     columns_gather.last()
 
-    gains = gain_ref[...].astype(jnp.float32)
+    gains = [
+        ref[...].astype(jnp.float32).reshape(1, width) for ref in (gm_ref, gf_ref, go_ref)
+    ]
     mixed = jnp.concatenate([cbuf[o] for o in range(device_count)], axis=1).astype(jnp.float32)
     stage = xbuf[...].reshape(total_rows, xbuf.shape[2])
-    after_mix = (stage[:, :width].astype(jnp.float32) + gains[0:1] * normalize(mixed)).astype(
+    after_mix = (stage[:, :width].astype(jnp.float32) + gains[0] * normalize(mixed)).astype(
         jnp.bfloat16
     )
     mix_rows[...] = after_mix.reshape(mix_rows.shape)
-    ffn_in = (normalize(after_mix.astype(jnp.float32)) * gains[1:2]).astype(jnp.bfloat16)
+    ffn_in = (normalize(after_mix.astype(jnp.float32)) * gains[1]).astype(jnp.bfloat16)
     norm_rows[...] = ffn_in.reshape(norm_rows.shape)
-    weight_copies[2].wait()
-    affinity = jax.nn.sigmoid(jnp.dot(ffn_in, router[...], preferred_element_type=jnp.float32))
+    weight_copies[1].wait()
+    affinity = jax.nn.sigmoid(
+        lax.dot_general(
+            ffn_in, router[...], (((1,), (1,)), ((), ())), preferred_element_type=jnp.float32
+        )
+    )
     hot = stage[:, width : width + affinity.shape[1]].astype(jnp.float32)
     chosen = affinity * hot
     lane = lax.broadcasted_iota(jnp.int32, chosen.shape, 1)
     mine = jnp.sum(jnp.where(lane == me, chosen, 0.0), axis=1, keepdims=True)
     mine = mine / jnp.sum(chosen, axis=1, keepdims=True) * routed_scale
-    for copy in weight_copies[3:6]:
+    for copy in weight_copies[2:5]:
         copy.wait()
     expert_out = swiglu(ffn_in, eg[...], eu[...], ed[...])
     scaled = (expert_out.astype(jnp.float32) * mine).astype(jnp.bfloat16)
@@ -471,7 +548,7 @@
             )
             copy.start()
             sends.append(copy)
-    for copy in weight_copies[6:9]:
+    for copy in weight_copies[5:8]:
         copy.wait()
     combined = routed + swiglu(norm_rows[me], sg[...], su[...], sd[...]).astype(jnp.float32)
     for step in reversed(order[:-1]):
@@ -486,14 +563,10 @@
         ).wait_recv()
         combined = combined + back[e].astype(jnp.float32)
     out_ref[...] = (
-        mix_rows[me].astype(jnp.float32) + gains[2:3] * normalize(combined)
+        mix_rows[me].astype(jnp.float32) + gains[2] * normalize(combined)
     ).astype(jnp.bfloat16)
     for copy in pending + sib_copies + sends:
         copy.wait_send()
-
-
-def width_of_head(flat, heads):
-    return flat.shape[1] // heads
 
 
 def local_fused(
@@ -527,21 +600,6 @@
     bits = (ep_count - 1).bit_length()
     grid_p = 2 ** ((bits + 1) // 2)
     grid_q = ep_count // grid_p
-    positions = lengths.astype(jnp.float32)
-    query_latent = jnp.einsum(
-        "shn,chn->shc", query_nope, absorb_key, preferred_element_type=jnp.float32
-    ).astype(jnp.bfloat16)
-    query_pe = rotate(query_rope.astype(jnp.float32), positions[:, None, None]).astype(jnp.bfloat16)
-    latent_new = normalize(new_latent.astype(jnp.float32)).astype(jnp.bfloat16)
-    key_new = rotate(new_rope.astype(jnp.float32), positions[:, None]).astype(jnp.bfloat16)
-    own_start = lax.axis_index("tp") * seq_count
-    own_routes = lax.dynamic_slice_in_dim(routes, own_start, seq_count, 0)
-    hot = jnp.any(
-        own_routes[:, :, None] == lax.iota(jnp.int32, 128)[None, None, :], axis=1
-    ).astype(jnp.bfloat16)
-    own = jnp.concatenate([hidden_in, hot], axis=1)
-    gains = jnp.stack([gain_mix, gain_ffn_in, gain_ffn_out])
-    value_flat = value_up.reshape(value_up.shape[0], -1)
     bf = jnp.bfloat16
     score_scale = (query_nope.shape[-1] + query_rope.shape[-1]) ** (-0.5)
     sends = (grid_p - 1) + grid_p * (grid_q - 1) + ep_count
@@ -549,10 +607,13 @@
     near = pl.BlockSpec(memory_space=pltpu.VMEM)
     dma = pltpu.SemaphoreType.DMA
     total_rows = device_count * seq_count
+    rope_rows = jnp.swapaxes(cache_rope, 1, 2)
+    router_rows = jnp.swapaxes(router, 0, 1)
+    absorb_rows = jnp.transpose(absorb_key, (1, 2, 0)).reshape(-1, latent)
+    own_shape = (seq_count, width + 128)
     weights = (
-        value_flat,
         out_proj,
-        router,
+        router_rows,
         expert_gate[0],
         expert_up[0],
         expert_down[0],
@@ -561,26 +622,23 @@
         shared_down,
     )
     operands = (
-        query_latent,
-        query_pe,
-        latent_new,
-        key_new,
+        hidden_in,
+        query_nope,
+        query_rope,
+        new_latent,
+        new_rope,
         lengths,
-        own,
+        jnp.swapaxes(routes, 0, 1),
+        gain_mix,
+        gain_ffn_in,
+        gain_ffn_out,
+        absorb_rows,
         cache_latent,
-        cache_rope,
-        value_flat,
-        out_proj,
-        gains,
-        router,
-    ) + weights[3:]
-    specs = (
-        [near] * 4
-        + [pl.BlockSpec(memory_space=pltpu.SMEM), near]
-        + [big] * 4
-        + [near]
-        + [big] * 7
-    )
+        rope_rows,
+        value_up,
+    ) + weights
+    scalar = pl.BlockSpec(memory_space=pltpu.SMEM)
+    specs = [near] * 5 + [scalar] * 2 + [near] * 3 + [big] * 12
     flops = 2 * total_rows * width * out_proj.shape[1]
     return pl.pallas_call(
         functools.partial(fused_kernel, grid_p, grid_q, score_scale),
@@ -589,11 +647,17 @@
         out_specs=near,
         scratch_shapes=[
             pltpu.VMEM(cache_latent.shape, bf),
-            pltpu.VMEM(cache_rope.shape, bf),
+            pltpu.VMEM(rope_rows.shape, bf),
+            pltpu.VMEM((latent, value_up.shape[1] * value_up.shape[2]), bf),
+            pltpu.VMEM(value_up.shape, jnp.float32),
+            pltpu.VMEM((seq_count * heads, latent), bf),
+            pltpu.VMEM((seq_count * heads, query_rope.shape[2]), bf),
+            pltpu.VMEM(absorb_rows.shape, bf),
+            pltpu.VMEM(value_up.shape, bf),
         ]
         + [pltpu.VMEM(w.shape, bf) for w in weights]
         + [
-            pltpu.VMEM((device_count,) + own.shape, bf),
+            pltpu.VMEM((device_count,) + own_shape, bf),
             pltpu.VMEM((device_count, seq_count, out_proj.shape[0]), bf),
             pltpu.VMEM((device_count, total_rows, out_proj.shape[1]), bf),
             pltpu.VMEM((seq_count * heads, latent), bf),
@@ -605,7 +669,7 @@
             pltpu.VMEM((ep_count, seq_count, width), bf),
             dma((seq_count,)),
             dma((seq_count,)),
-            dma((len(weights),)),
+            dma((len(weights) + 2,)),
             dma((3, sends)),
             dma((3, device_count)),
             dma((ep_count,)),

time: 65.8 us -> 49.4 us (0.75)
  local copies, waits for them, and re-layouts: 11 us -> 1.38 us
  other arithmetic: 8.02 us -> 0 us
  Pallas kernels: 45.1 us -> 47.8 us
  matrix products: 0.92 us -> 0 us
    unnamed x8 -> x1, local copies, waits for them, and re-layouts: 7.48 us -> 1.38 us
    convert_element_type x5 -> x0, other arithmetic: 3.47 us -> none  [the longest x1 1.35 us: local_fused(): latent_new = normalize(new_latent.astype(jnp.float32)).astype(jnp.bfloat16)]
    concatenate x3 -> x0, other arithmetic: 2.73 us -> none  [the longest x2 1.37 us: rotate(): jnp.concatenate([first_half * cosine - second_half * sine_table, first_ha...]
    pallas_call x1, Pallas kernels: 45.1 us -> 47.8 us  [local_fused(): pl.pallas_call(functools.partial(fused_kernel, grid_p, grid_q, score_scal...]
    another operation x3 -> x0, local copies, waits for them, and re-layouts: 2.08 us -> none  [local_fused(): gains = jnp.stack([gain_mix, gain_ffn_in, gain_ffn_out])]
    dot_general x1 -> x0, matrix products: 0.92 us -> none  [local_fused(): jnp.einsum('shn,chn->shc', query_nope, absorb_key, preferred_element_type...]
    reduce_sum x1 -> x0, other arithmetic: 0.89 us -> none  [normalize(): jnp.mean(values * values, axis=-1, keepdims=True) + norm_eps]
    another operation x3 -> x0, other arithmetic: 0.83 us -> none  [the longest x1 0.63 us: local_fused(): gains = jnp.stack([gain_mix, gain_ffn_in, gain_ffn_out])]
where the time goes in v2:
time: 49.4 us; the launch traced here: 49.2 us
  Pallas kernels  47.8 us (97%)
  local copies, waits for them, and re-layouts  1.38 us (3%)
    pallas_call x1, Pallas kernels, local_fused(): pl.pallas_call(functools.partial(fused_kernel, grid_p, grid_q, score_scal...  47.8 us
    unnamed x1, local copies, waits for them, and re-layouts  1.38 us

profile of v2, /device:TPU:0, one launch (start us, length us, event | category | flops | bytes accessed | tf_op | source)
XLA Modules:
  0.0 49.2 jit_solution(9942930677677833378)
XLA Ops:
  0.0 47.8 %layer_step.1 = bf16[8,2048]{1,0:T(8,128)(2,1)} custom-call(bf16[8,2048]{1,0:T(8,128)(2,1)} %hidden_ref.1, bf16[8,16,64]{2,1,0:T(8,128)(2,1)} %qn_ref.1, bf16[8,16,32]{2,1,0:T(8,128)(2,1)} %qr_ref.1, bf16[8,256]{1,0:T(8,128)(2,1)} %nl_ref.1, bf16[8,32]{1,0:T(8,128)(2,1)} %nr_ref.1, s32[8]{0:T(128)} %len_ref.1, s32[6,16]{1,0:T(8,128)} %bitcast.15, ...), custom_call_target="tpu_custom_call" | custom-call | flops 67108864 | bytes 16777216 | tf_op jit(solution)/shard_map/layer_step/pallas_call | solution.py:643
  47.8 1.4 %copy.24 = bf16[8,2048]{1,0:T(8,128)(2,1)} copy(bf16[8,2048]{1,0:T(8,128)(2,1)} %layer_step.1) | data formatting | bytes 65536

commit v3 on v2

--- a/solution.py
+++ b/solution.py
@@ -313,6 +313,69 @@
             marks = jnp.where((mark_row == s) & (mark_lane == expert), 1.0, marks)
     xbuf[me, :, width:] = marks.astype(jnp.bfloat16)
 
+    line_steps = list(range(1, grid_p))
+    pending = []
+
+    class Gather:
+        def __init__(self, buf, which):
+            self.buf, self.which, self.count = buf, which, 0
+
+        def send(self, slot, target):
+            copy = pltpu.make_async_remote_copy(
+                src_ref=self.buf.at[slot],
+                dst_ref=self.buf.at[slot],
+                send_sem=ag_send.at[self.which, self.count],
+                recv_sem=ag_recv.at[self.which, slot],
+                device_id=target,
+                device_id_type=pl.DeviceIdType.MESH,
+            )
+            copy.start()
+            pending.append(copy)
+            self.count += 1
+
+        def arrive(self, slot):
+            pltpu.make_async_remote_copy(
+                src_ref=self.buf.at[slot],
+                dst_ref=self.buf.at[slot],
+                send_sem=ag_send.at[self.which, 0],
+                recv_sem=ag_recv.at[self.which, slot],
+                device_id=sibling,
+                device_id_type=pl.DeviceIdType.MESH,
+            ).wait_recv()
+
+        def line(self, step):
+            return (p + step) % grid_p
+
+        def first(self):
+            for step in sorted(line_steps, key=lambda v: -min(v, grid_p - v)):
+                self.send(me, device(self.line(step) * grid_q + q, me_t))
+            for turn in range(1, grid_q):
+                self.send(me, device(p * grid_q + (q + turn) % grid_q, me_t))
+            self.send(me, sibling)
+
+        def second(self):
+            for step in sorted(line_steps, key=lambda v: min(v, grid_p - v)):
+                slot = (self.line(step) * grid_q + q) * 2 + me_t
+                self.arrive(slot)
+                for turn in range(1, grid_q):
+                    self.send(slot, device(p * grid_q + (q + turn) % grid_q, me_t))
+                self.send(slot, sibling)
+
+        def third(self):
+            for step in sorted([0] + line_steps, key=lambda v: min(v, grid_p - v)):
+                for turn in range(1, grid_q):
+                    slot = (self.line(step) * grid_q + (q + turn) % grid_q) * 2 + me_t
+                    self.arrive(slot)
+                    self.send(slot, sibling)
+
+        def last(self):
+            for e in range(ep_count):
+                self.arrive(e * 2 + other_t)
+
+    rows_gather = Gather(xbuf, 0)
+    pl.semaphore_wait(barrier, ep_count)
+    rows_gather.first()
+
     half = rope // 2
     turn_row = lax.broadcasted_iota(jnp.int32, (seq_count, rope), 0)
     turn_lane = lax.broadcasted_iota(jnp.int32, (seq_count, rope), 1)
@@ -356,65 +419,6 @@
     ql_ref[...] = jnp.dot(spread_query, ab[...], preferred_element_type=jnp.float32).astype(
         jnp.bfloat16
     )
-
-    line_steps = list(range(1, grid_p))
-    pending = []
-
-    class Gather:
-        def __init__(self, buf, which):
-            self.buf, self.which, self.count = buf, which, 0
-
-        def send(self, slot, target):
-            copy = pltpu.make_async_remote_copy(
-                src_ref=self.buf.at[slot],
-                dst_ref=self.buf.at[slot],
-                send_sem=ag_send.at[self.which, self.count],
-                recv_sem=ag_recv.at[self.which, slot],
-                device_id=target,
-                device_id_type=pl.DeviceIdType.MESH,
-            )
-            copy.start()
-            pending.append(copy)
-            self.count += 1
-
-        def arrive(self, slot):
-            pltpu.make_async_remote_copy(
-                src_ref=self.buf.at[slot],
-                dst_ref=self.buf.at[slot],
-                send_sem=ag_send.at[self.which, 0],
-                recv_sem=ag_recv.at[self.which, slot],
-                device_id=sibling,
-                device_id_type=pl.DeviceIdType.MESH,
-            ).wait_recv()
-
-        def line(self, step):
-            return (p + step) % grid_p
-
-        def first(self):
-            for step in sorted(line_steps, key=lambda v: -min(v, grid_p - v)):
-                self.send(me, device(self.line(step) * grid_q + q, me_t))
-            for turn in range(1, grid_q):
-                self.send(me, device(p * grid_q + (q + turn) % grid_q, me_t))
-            self.send(me, sibling)
-
-        def second(self):
-            for step in sorted(line_steps, key=lambda v: min(v, grid_p - v)):
-                slot = (self.line(step) * grid_q + q) * 2 + me_t
-                self.arrive(slot)
-                for turn in range(1, grid_q):
-                    self.send(slot, device(p * grid_q + (q + turn) % grid_q, me_t))
-                self.send(slot, sibling)
-
-        def third(self):
-            for step in sorted([0] + line_steps, key=lambda v: min(v, grid_p - v)):
-                for turn in range(1, grid_q):
-                    slot = (self.line(step) * grid_q + (q + turn) % grid_q) * 2 + me_t
-                    self.arrive(slot)
-                    self.send(slot, sibling)
-
-        def last(self):
-            for e in range(ep_count):
-                self.arrive(e * 2 + other_t)
 
     context = cl.shape[1]
     key_index = lax.broadcasted_iota(jnp.int32, (heads, context), 1)
@@ -445,21 +449,16 @@
         weighted = weighted + new_weight.astype(jnp.bfloat16).astype(jnp.float32) * new_row
         lat[s * heads : (s + 1) * heads, :] = (weighted / weight_total).astype(jnp.bfloat16)
 
-    rows_gather = Gather(xbuf, 0)
-    cut_a, cut_b = seq_count // 2, seq_count - seq_count // 4
-    for s in range(cut_a):
-        attend(s)
     early_copies[1].wait()
     value_dim = vraw.shape[2]
     wide_up[...] = vraw[...].astype(jnp.float32)
     for h in range(heads):
         vup[:, h * value_dim : (h + 1) * value_dim] = wide_up[:, h, :].astype(jnp.bfloat16)
-    pl.semaphore_wait(barrier, ep_count)
-    rows_gather.first()
-    for s in range(cut_a, cut_b):
+    cut_a = seq_count // 2
+    for s in range(cut_a):
         attend(s)
     rows_gather.second()
-    for s in range(cut_b, seq_count):
+    for s in range(cut_a, seq_count):
         attend(s)
 
     spread = jnp.dot(lat[...], vup[...], preferred_element_type=jnp.float32)

time: 49.4 us -> 47.2 us (0.955)
  Pallas kernels: 47.8 us -> 45.6 us
    pallas_call x1, Pallas kernels: 47.8 us -> 45.6 us  [local_fused(): pl.pallas_call(functools.partial(fused_kernel, grid_p, grid_q, score_scal...]
where the time goes in v3:
time: 47.2 us; the launch traced here: 47 us
  Pallas kernels  45.6 us (97%)
  local copies, waits for them, and re-layouts  1.38 us (3%)
    pallas_call x1, Pallas kernels, local_fused(): pl.pallas_call(functools.partial(fused_kernel, grid_p, grid_q, score_scal...  45.6 us
    unnamed x1, local copies, waits for them, and re-layouts  1.38 us

profile of v3, /device:TPU:0, one launch (start us, length us, event | category | flops | bytes accessed | tf_op | source)
XLA Modules:
  0.0 47.0 jit_solution(5468926311698768754)
XLA Ops:
  0.0 45.6 %layer_step.1 = bf16[8,2048]{1,0:T(8,128)(2,1)} custom-call(bf16[8,2048]{1,0:T(8,128)(2,1)} %hidden_ref.1, bf16[8,16,64]{2,1,0:T(8,128)(2,1)} %qn_ref.1, bf16[8,16,32]{2,1,0:T(8,128)(2,1)} %qr_ref.1, bf16[8,256]{1,0:T(8,128)(2,1)} %nl_ref.1, bf16[8,32]{1,0:T(8,128)(2,1)} %nr_ref.1, s32[8]{0:T(128)} %len_ref.1, s32[6,16]{1,0:T(8,128)} %bitcast.15, ...), custom_call_target="tpu_custom_call" | custom-call | flops 67108864 | bytes 16777216 | tf_op jit(solution)/shard_map/layer_step/pallas_call | solution.py:642
  45.6 1.4 %copy.24 = bf16[8,2048]{1,0:T(8,128)(2,1)} copy(bf16[8,2048]{1,0:T(8,128)(2,1)} %layer_step.1) | data formatting | bytes 65536
